TPU v7x, 32 devices: a whole 2x2x4 slice. The times are simulated.
32 devices in a mesh: ep: 8 (over z, x), tp: 4 (over y, core).
Axes of the slice: x: 2, y: 2, z: 4, core: 2. Of those that a mesh axis runs over, the one named last changes fastest.
Arguments:
- tokens: bfloat16 [32, 2048], P(('ep', 'tp')), may hold values from -6 to 6
- norm_gain: float32 [2048], replicated, may hold values from 0.1 to 1.9
- w_query: bfloat16 [2048, 4096], P('ep', 'tp'), may hold values from -0.125 to 0.125
- w_key: bfloat16 [2048, 512], P('ep', 'tp'), may hold values from -0.125 to 0.125
- w_value: bfloat16 [2048, 512], P('ep', 'tp'), may hold values from -0.125 to 0.125
- key_cache: bfloat16 [32, 1024, 512], P(('ep', 'tp')), may hold values from -900 to 900
- value_cache: bfloat16 [32, 1024, 512], P(('ep', 'tp')), may hold values from -6 to 6
- lengths: int32 [32], P(('ep', 'tp')), may hold values from 512 to 1023, as said below
- diff_lambda: float32 [16], replicated, may hold values from 0.3 to 0.8
- head_gain: float32 [256], replicated, may hold values from 0.1 to 1.9
- w_out: bfloat16 [4096, 2048], P('tp', 'ep'), may hold values from -0.09375 to 0.09375
- ffn_gain: float32 [2048], replicated, may hold values from 0.1 to 1.9
- routing: int32 [32, 2], P('ep'), may hold values from 0 to 7, all different within a row; in each aligned block of 4 rows (0 to 3, 4 to 7, ...) at most 4 rows name the same one
- route_weight: float32 [32, 2], P('ep'), may hold values from 0.2 to 1
- w_gate: bfloat16 [8, 2048, 3584], P('ep', None, 'tp'), may hold values from -0.125 to 0.125
- w_up: bfloat16 [8, 2048, 3584], P('ep', None, 'tp'), may hold values from -0.125 to 0.125
- w_down: bfloat16 [8, 3584, 2048], P('ep', 'tp'), may hold values from -0.09375 to 0.09375
Outputs:
- result: bfloat16 [32, 2048], P(('ep', 'tp'))
- new_keys: bfloat16 [32, 512], P(('ep', 'tp'))
- new_values: bfloat16 [32, 512], P(('ep', 'tp'))
Inputs may be any that keep to these rules, and one draw needn't show every extreme that they name: Each sequence's new token sits at position lengths[s], just after its valid cached positions. `routing`: each row names 2 different experts. In each aligned block of 4 rows (one ep index's sequences) no expert is named by more than 4 rows.
All inputs are finite; a program needn't handle non-finite values.
Results may differ from a plain program's by a relative error of at most 0.017.
Values may be sent and summed in bfloat16 or wider, within the bound.
A program may use at most 64 MiB of HBM per device.

v0:
```python
import functools

import jax
import jax.numpy as jnp
from jax import lax
from jax.experimental import pallas as pl
from jax.experimental.pallas import tpu as pltpu
from jax.sharding import PartitionSpec as P

HEADS = 16
KV_HEADS = 2
HEAD_QK = 128
HEAD_V = 256
TOPK = 2
LEN = 1024
SEQ_DEV = 1


NORM_EPS = 1e-05
HEAD_EPS = 0.01
HEAD_SCALE = 0.8


def rms_scale(values, gain_row, floor_add):
    mean_sq = jnp.mean(values * values, axis=-1, keepdims=True)
    return values * lax.rsqrt(mean_sq + floor_add) * gain_row


def attend(queries, key_rows, value_rows, key_cache, value_cache, lengths, diff_lambda, head_gain):
    row_count = queries.shape[0]
    repeat = HEADS // KV_HEADS
    queries = queries.reshape(row_count, KV_HEADS, repeat, 2, HEAD_QK)
    key_rows = key_rows.reshape(row_count, KV_HEADS, 2, HEAD_QK)
    value_rows = value_rows.reshape(row_count, KV_HEADS, HEAD_V)
    cache_keys = key_cache.reshape(row_count, LEN, KV_HEADS, 2, HEAD_QK)
    cache_vals = value_cache.reshape(row_count, LEN, KV_HEADS, HEAD_V)
    score_scale = HEAD_QK ** (-0.5)
    cached = (
        jnp.einsum("sgrcd,slgcd->sgrcl", queries, cache_keys, preferred_element_type=jnp.float32)
        * score_scale
    )
    own_score = (
        jnp.einsum("sgrcd,sgcd->sgrc", queries, key_rows, preferred_element_type=jnp.float32)
        * score_scale
    )
    in_range = jnp.arange(LEN)[None, :] < lengths[:, None]
    cached = jnp.where(in_range[:, None, None, None, :], cached, -jnp.inf)
    row_peak = jnp.maximum(jnp.max(cached, axis=-1), own_score)
    cached_w = jnp.exp(cached - row_peak[..., None])
    own_w = jnp.exp(own_score - row_peak)
    row_total = jnp.sum(cached_w, axis=-1) + own_w
    cached_w = cached_w / row_total[..., None]
    own_w = own_w / row_total
    lam_heads = diff_lambda.reshape(1, KV_HEADS, repeat)
    mix_cached = (cached_w[:, :, :, 0] - lam_heads[..., None] * cached_w[:, :, :, 1]).astype(
        jnp.bfloat16
    )
    mix_own = (own_w[..., 0] - lam_heads * own_w[..., 1]).astype(jnp.bfloat16)
    head_raw = jnp.einsum(
        "sgrl,slgv->sgrv", mix_cached, cache_vals, preferred_element_type=jnp.float32
    )
    head_raw = (
        head_raw
        + mix_own.astype(jnp.float32)[..., None] * value_rows.astype(jnp.float32)[:, :, None, :]
    )
    head_out = rms_scale(head_raw, head_gain, HEAD_EPS) * HEAD_SCALE
    return head_out.astype(jnp.bfloat16).reshape(row_count, HEADS * HEAD_V)


def body(
    tokens,
    norm_gain,
    w_query,
    w_key,
    w_value,
    key_cache,
    value_cache,
    lengths,
    diff_lambda,
    head_gain,
    w_out,
    ffn_gain,
    routing,
    route_weight,
    w_gate,
    w_up,
    w_down,
):
    group_tokens = lax.all_gather(tokens, "tp", axis=0, tiled=True)
    normed = rms_scale(group_tokens.astype(jnp.float32), norm_gain, NORM_EPS).astype(jnp.bfloat16)
    blocks = lax.all_to_all(normed, "ep", split_axis=1, concat_axis=0, tiled=True)
    query_term = jnp.dot(blocks, w_query, preferred_element_type=jnp.float32)
    key_term = jnp.dot(blocks, w_key, preferred_element_type=jnp.float32)
    value_term = jnp.dot(blocks, w_value, preferred_element_type=jnp.float32)
    query_sum, key_sum, value_sum = (
        lax.psum_scatter(query_term, "ep", scatter_dimension=0, tiled=True),
        lax.psum_scatter(key_term, "ep", scatter_dimension=0, tiled=True),
        lax.psum_scatter(value_term, "ep", scatter_dimension=0, tiled=True),
    )
    queries = query_sum.astype(jnp.bfloat16)
    keys_made = key_sum.astype(jnp.bfloat16)
    values_made = value_sum.astype(jnp.bfloat16)
    own_query, new_keys, new_values = (
        lax.all_to_all(queries, "tp", split_axis=0, concat_axis=1, tiled=True),
        lax.all_to_all(keys_made, "tp", split_axis=0, concat_axis=1, tiled=True),
        lax.all_to_all(values_made, "tp", split_axis=0, concat_axis=1, tiled=True),
    )
    head_out = attend(
        own_query, new_keys, new_values, key_cache, value_cache, lengths, diff_lambda, head_gain
    )
    head_rows = lax.all_to_all(head_out, "tp", split_axis=1, concat_axis=0, tiled=True)
    partial_out = jnp.dot(
        head_rows,
        lax.all_gather(w_out, "ep", axis=1, tiled=True),
        preferred_element_type=jnp.float32,
    )
    attn_sum = lax.psum_scatter(
        partial_out.astype(jnp.bfloat16), "tp", scatter_dimension=0, tiled=True
    ).astype(jnp.float32)
    residual = tokens.astype(jnp.float32) + attn_sum
    ffn_in = rms_scale(residual, ffn_gain, NORM_EPS).astype(jnp.bfloat16)
    group_in = lax.all_gather(ffn_in, "tp", axis=0, tiled=True)
    experts = lax.axis_size("ep")
    capacity = 8 * SEQ_DEV * lax.axis_size("tp") // experts
    group_rows = group_in.shape[0]
    picks = routing.reshape(-1)
    choose = (picks[:, None] == jnp.arange(experts)[None, :]).astype(jnp.int32)
    earlier = jnp.cumsum(choose, axis=0) - choose
    slot_in = jnp.sum(earlier * choose, axis=1)
    slot_ids = (picks * capacity + slot_in).reshape(group_rows, TOPK)
    slot_hit = slot_ids[:, :, None] == jnp.arange(experts * capacity)[None, None, :]
    dispatch = jnp.sum(slot_hit, axis=1).astype(jnp.bfloat16)
    outgoing = jnp.einsum(
        "rj,rd->jd", dispatch, group_in, preferred_element_type=jnp.float32
    ).astype(jnp.bfloat16)
    outgoing = outgoing.reshape(experts, capacity, group_in.shape[1])
    arrived = lax.all_to_all(outgoing, "ep", split_axis=0, concat_axis=0, tiled=True)
    sources, slot_count, feat_dim = arrived.shape
    flat_rows = arrived.reshape(sources * slot_count, feat_dim)
    gate_pre = jnp.dot(flat_rows, w_gate[0], preferred_element_type=jnp.float32)
    up_pre = jnp.dot(flat_rows, w_up[0], preferred_element_type=jnp.float32)
    hidden = (jax.nn.silu(gate_pre) * up_pre).astype(jnp.bfloat16)
    partial_down = jnp.dot(hidden, w_down[0], preferred_element_type=jnp.float32)
    summed = lax.psum_scatter(
        partial_down.astype(jnp.bfloat16), "tp", scatter_dimension=1, tiled=True
    )
    expert_rows = summed.reshape(sources, slot_count, summed.shape[1])
    returned = lax.all_to_all(expert_rows, "ep", split_axis=0, concat_axis=0, tiled=True)
    combine = jnp.sum(slot_hit.astype(jnp.float32) * route_weight[:, :, None], axis=1)
    flat_back = returned.reshape(experts * capacity, returned.shape[2]).astype(jnp.float32)
    moe_cols = jnp.dot(combine, flat_back, precision=lax.Precision.HIGHEST)
    moe_own = lax.all_to_all(moe_cols, "tp", split_axis=0, concat_axis=1, tiled=True)
    return ((residual + moe_own).astype(jnp.bfloat16), new_keys, new_values)


F32 = jnp.float32
BF16 = jnp.bfloat16
LANES = 128


def fused_kernel(
    ep_size,
    tp_size,
    tok_ref,
    norm_gain_ref,
    wq_hbm,
    wk_hbm,
    wv_hbm,
    kc_hbm,
    vc_hbm,
    len_ref,
    lam_ref,
    head_gain_ref,
    wo_hbm,
    ffn_gain_ref,
    routing_ref,
    rweight_ref,
    wg_hbm,
    wu_hbm,
    wd_hbm,
    out_ref,
    nk_ref,
    nv_ref,
    wqkv,
    kc,
    vc,
    wo,
    wg,
    wu,
    wd,
    a_send,
    a_recv,
    b_send,
    b_recv,
    c_send,
    c_recv,
    d_send,
    d_recv,
    r_send,
    r_recv,
    e_send,
    e_recv,
    stage,
    raw_keep,
    res_stage,
    load_sems,
    send_sems,
    recv_sems,
):
    n_dev = ep_size * tp_size
    my_ep = lax.axis_index("ep")
    my_tp = lax.axis_index("tp")
    me = my_ep * tp_size + my_tp
    width = tok_ref.shape[1]
    feat = width // ep_size
    pieces = feat // LANES
    q_cols = wq_hbm.shape[1]
    q_rows = q_cols // LANES
    repeat = HEADS // KV_HEADS

    loads = [
        (wq_hbm, wqkv.at[:, pl.ds(0, q_cols)]),
        (wk_hbm, wqkv.at[:, pl.ds(q_cols, LANES)]),
        (wv_hbm, wqkv.at[:, pl.ds(q_cols + LANES, LANES)]),
        (kc_hbm.at[0], kc),
        (vc_hbm.at[0], vc),
        (wo_hbm, wo),
        (wg_hbm.at[0], wg),
        (wu_hbm.at[0], wu),
        (wd_hbm.at[0], wd),
    ]
    loads = [
        pltpu.make_async_copy(src, dst, load_sems.at[i]) for i, (src, dst) in enumerate(loads)
    ]
    for load in loads:
        load.start()

    barrier = pltpu.get_barrier_semaphore()

    def greet(step, carry):
        to = lax.rem(me + step, n_dev)
        pl.semaphore_signal(
            barrier,
            inc=1,
            device_id={"ep": to // tp_size, "tp": lax.rem(to, tp_size)},
            device_id_type=pl.DeviceIdType.MESH,
        )
        return carry

    lax.fori_loop(1, n_dev, greet, 0)

    def exchange(phase, count, source_of, target, place, device_of, my_place):
        own = pltpu.make_async_copy(source_of(my_place), target.at[place], recv_sems.at[phase])
        own.start()

        def send(step, carry):
            to = lax.rem(my_place + step, count)
            pltpu.make_async_remote_copy(
                src_ref=source_of(to),
                dst_ref=target.at[place],
                send_sem=send_sems.at[phase],
                recv_sem=recv_sems.at[phase],
                device_id=device_of(to),
                device_id_type=pl.DeviceIdType.MESH,
            ).start()
            return carry

        lax.fori_loop(1, count, send, 0)

    def arrive(phase, target):
        pltpu.make_async_copy(target, target, recv_sems.at[phase]).wait()

    def flushed(phase, count, target):
        part = target.at[pl.ds(0, count - 1)]
        pltpu.make_async_copy(part, part, send_sems.at[phase]).wait()

    def any_device(to):
        return {"ep": to // tp_size, "tp": lax.rem(to, tp_size)}

    tok = tok_ref[...].astype(F32)
    mean_sq = jnp.mean(tok * tok, axis=-1, keepdims=True)
    normed = tok * lax.rsqrt(mean_sq + NORM_EPS) * norm_gain_ref[...]
    for e in range(ep_size):
        for p in range(pieces):
            cols = slice(e * feat + p * LANES, e * feat + (p + 1) * LANES)
            stage[e * 8 + p : e * 8 + p + 1, :] = normed[:, cols]
            stage[e * 8 + pieces + p : e * 8 + pieces + p + 1, :] = tok[:, cols]
    a_send[...] = stage[0 : ep_size * 8, :].astype(BF16).reshape(ep_size, 8, LANES)
    pl.semaphore_wait(barrier, n_dev - 1)
    exchange(0, n_dev, lambda to: a_send.at[to // tp_size], a_recv, me, any_device, me)
    arrive(0, a_recv)
    stage[0 : n_dev * 8, :] = a_recv[...].astype(F32).reshape(n_dev * 8, LANES)
    blocks = jnp.concatenate(
        [stage[pl.ds(p, n_dev, stride=8), :] for p in range(pieces)], axis=1
    ).astype(BF16)
    for p in range(pieces):
        raw_keep[:, p * LANES : (p + 1) * LANES] = stage[pl.ds(pieces + p, n_dev, stride=8), :]

    for i in range(3):
        loads[i].wait()
    proj = jnp.dot(blocks, wqkv[...], preferred_element_type=F32)
    for j in range(q_rows + 2):
        stage[pl.ds(j, n_dev, stride=16), :] = proj[:, j * LANES : (j + 1) * LANES]
    b_send[...] = stage[...].astype(BF16).reshape(n_dev, 16, LANES)
    exchange(1, n_dev, lambda to: b_send.at[to], b_recv, me, any_device, me)
    arrive(1, b_recv)
    q_parts, k_parts, v_parts = [], [], []
    for t in range(tp_size):
        total = b_recv[t].astype(F32)
        for e in range(1, ep_size):
            total = total + b_recv[e * tp_size + t].astype(F32)
        q_parts.append(total[0:q_rows])
        key_row = total[q_rows : q_rows + 1].astype(BF16)
        value_row = total[q_rows + 1 : q_rows + 2].astype(BF16)
        nk_ref[:, t * LANES : (t + 1) * LANES] = key_row
        nv_ref[:, t * LANES : (t + 1) * LANES] = value_row
        k_parts.append(key_row.astype(F32))
        v_parts.append(value_row.astype(F32))
    q_all = jnp.concatenate(q_parts, axis=0).astype(BF16)

    loads[3].wait()
    loads[4].wait()
    rows = 2 * repeat
    length = len_ref[0]
    positions = kc.shape[0]
    first_map = lax.rem(lax.broadcasted_iota(jnp.int32, (rows, LANES), 0), 2) == 0
    first_wide = lax.rem(lax.broadcasted_iota(jnp.int32, (rows, positions), 0), 2) == 0
    valid = lax.broadcasted_iota(jnp.int32, (rows, positions), 1) < length
    head_at = lax.broadcasted_iota(jnp.int32, (rows, LANES), 0) // 2
    scale = HEAD_QK ** (-0.5)
    contract = (((1,), (1,)), ((), ()))
    for g in range(KV_HEADS):
        q = q_all[g * rows : (g + 1) * rows]
        base = g * 2 * HEAD_QK
        s0 = lax.dot_general(
            q, kc[:, base : base + HEAD_QK], contract, preferred_element_type=F32
        )
        s1 = lax.dot_general(
            q, kc[:, base + HEAD_QK : base + 2 * HEAD_QK], contract, preferred_element_type=F32
        )
        score = jnp.where(valid, jnp.where(first_wide, s0, s1) * scale, -jnp.inf)
        q32 = q.astype(F32)
        own = jnp.sum(
            q32 * jnp.where(first_map, k_parts[2 * g], k_parts[2 * g + 1]), axis=-1, keepdims=True
        ) * scale
        peak = jnp.maximum(jnp.max(score, axis=-1, keepdims=True), own)
        weight = jnp.exp(score - peak)
        own_weight = jnp.exp(own - peak)
        norm = jnp.sum(weight, axis=-1, keepdims=True) + own_weight
        weight = weight / norm
        own_weight = jnp.broadcast_to(own_weight / norm, (rows, LANES))
        lam = jnp.zeros((rows, LANES), F32)
        for r in range(repeat):
            lam = jnp.where(head_at == r, lam_ref[g * repeat + r], lam)
        mix = (weight - lam[:, 0:1] * pltpu.roll(weight, rows - 1, 0)).astype(BF16)
        mix_own = (own_weight - lam * pltpu.roll(own_weight, rows - 1, 0)).astype(BF16).astype(F32)
        raw = jnp.dot(
            mix, vc[:, g * HEAD_V : (g + 1) * HEAD_V], preferred_element_type=F32
        )
        raw = raw + jnp.concatenate(
            [mix_own * v_parts[2 * g], mix_own * v_parts[2 * g + 1]], axis=1
        )
        mean_sq = jnp.mean(raw * raw, axis=-1, keepdims=True)
        head = raw * lax.rsqrt(mean_sq + HEAD_EPS) * head_gain_ref[...] * HEAD_SCALE
        for half in range(2):
            at = half * KV_HEADS * rows + g * rows
            stage[at : at + rows, :] = head[:, half * LANES : (half + 1) * LANES]
    heads_dev = HEADS // tp_size
    halves = [stage[pl.ds(half * KV_HEADS * rows, HEADS, stride=2), :] for half in range(2)]
    for t in range(tp_size):
        for half in range(2):
            at = t * 8 + half * heads_dev
            stage[at : at + heads_dev, :] = halves[half][t * heads_dev : (t + 1) * heads_dev]
    c_send[...] = stage[0 : tp_size * 8, :].astype(BF16).reshape(tp_size, 8, LANES)
    exchange(2, n_dev, lambda to: c_send.at[lax.rem(to, tp_size)], c_recv, me, any_device, me)
    arrive(2, c_recv)

    stage[0 : n_dev * 8, :] = c_recv[...].astype(F32).reshape(n_dev * 8, LANES)
    lhs = jnp.concatenate(
        [
            stage[pl.ds(half * heads_dev + r, n_dev, stride=8), :]
            for r in range(heads_dev)
            for half in range(2)
        ],
        axis=1,
    ).astype(BF16)
    loads[5].wait()
    d_send[...] = jnp.dot(lhs, wo[...], preferred_element_type=F32).astype(BF16)
    exchange(3, tp_size, lambda to: d_send, d_recv, my_tp, lambda to: {"tp": to}, my_tp)
    arrive(3, d_recv)
    total = raw_keep[...]
    for t in range(tp_size):
        total = total + d_recv[t].astype(F32)
    r_send[...] = total.astype(BF16)
    exchange(4, ep_size, lambda to: r_send, r_recv, my_ep, lambda to: {"ep": to}, my_ep)
    arrive(4, r_recv)
    residual = jnp.concatenate([r_recv[e].astype(F32) for e in range(ep_size)], axis=1)
    tile_rows = width // LANES
    for j in range(tile_rows):
        res_stage[pl.ds(j, n_dev, stride=tile_rows), :] = residual[:, j * LANES : (j + 1) * LANES]
    mean_sq = jnp.mean(residual * residual, axis=-1, keepdims=True)
    ffn_in = (residual * lax.rsqrt(mean_sq + NORM_EPS) * ffn_gain_ref[...]).astype(BF16)

    loads[6].wait()
    gate = jnp.dot(ffn_in, wg[...], preferred_element_type=F32)
    loads[7].wait()
    up = jnp.dot(ffn_in, wu[...], preferred_element_type=F32)
    hidden = (gate / (1.0 + jnp.exp(-gate)) * up).astype(BF16)
    loads[8].wait()
    down = jnp.dot(hidden, wd[...], preferred_element_type=F32)
    for j in range(tile_rows):
        stage[pl.ds(j, n_dev, stride=tile_rows), :] = down[:, j * LANES : (j + 1) * LANES]
    e_send[...] = stage[...].astype(BF16).reshape(n_dev, tile_rows, LANES)
    exchange(5, n_dev, lambda to: e_send.at[to], e_recv, me, any_device, me)
    arrive(5, e_recv)
    result = res_stage[pl.ds(me * tile_rows, tile_rows), :]
    for e in range(ep_size):
        share = jnp.float32(0.0)
        for k in range(TOPK):
            share = share + jnp.where(routing_ref[my_tp, k] == e, rweight_ref[my_tp, k], 0.0)
        total = e_recv[e * tp_size].astype(F32)
        for t in range(1, tp_size):
            total = total + e_recv[e * tp_size + t].astype(F32)
        result = result + total.astype(BF16).astype(F32) * share
    for j in range(tile_rows):
        out_ref[:, j * LANES : (j + 1) * LANES] = result[j : j + 1].astype(BF16)

    flushed(0, n_dev, a_recv)
    flushed(1, n_dev, b_recv)
    flushed(2, n_dev, c_recv)
    flushed(3, tp_size, d_recv)
    flushed(4, ep_size, r_recv)
    flushed(5, n_dev, e_recv)


def fused_body(
    tokens,
    norm_gain,
    w_query,
    w_key,
    w_value,
    key_cache,
    value_cache,
    lengths,
    diff_lambda,
    head_gain,
    w_out,
    ffn_gain,
    routing,
    route_weight,
    w_gate,
    w_up,
    w_down,
):
    ep_size, tp_size = lax.axis_size("ep"), lax.axis_size("tp")
    n_dev = ep_size * tp_size
    width = tokens.shape[1]
    feat = width // ep_size
    vmem = pl.BlockSpec(memory_space=pltpu.VMEM)
    smem = pl.BlockSpec(memory_space=pltpu.SMEM)
    hbm = pl.BlockSpec(memory_space=pl.ANY)
    tile_rows = width // LANES
    proj_cols = w_query.shape[1] + w_key.shape[1] + w_value.shape[1]
    scratch = [
        pltpu.VMEM((feat, proj_cols), BF16),
        pltpu.VMEM(key_cache.shape[1:], BF16),
        pltpu.VMEM(value_cache.shape[1:], BF16),
        pltpu.VMEM(w_out.shape, BF16),
        pltpu.VMEM(w_gate.shape[1:], BF16),
        pltpu.VMEM(w_up.shape[1:], BF16),
        pltpu.VMEM(w_down.shape[1:], BF16),
        pltpu.VMEM((ep_size, 8, LANES), BF16),
        pltpu.VMEM((n_dev, 8, LANES), BF16),
        pltpu.VMEM((n_dev, 16, LANES), BF16),
        pltpu.VMEM((n_dev, 16, LANES), BF16),
        pltpu.VMEM((tp_size, 8, LANES), BF16),
        pltpu.VMEM((n_dev, 8, LANES), BF16),
        pltpu.VMEM((n_dev, feat), BF16),
        pltpu.VMEM((tp_size, n_dev, feat), BF16),
        pltpu.VMEM((n_dev, feat), BF16),
        pltpu.VMEM((ep_size, n_dev, feat), BF16),
        pltpu.VMEM((n_dev, tile_rows, LANES), BF16),
        pltpu.VMEM((n_dev, tile_rows, LANES), BF16),
        pltpu.VMEM((n_dev * 16, LANES), F32),
        pltpu.VMEM((n_dev, feat), F32),
        pltpu.VMEM((n_dev * tile_rows, LANES), F32),
        pltpu.SemaphoreType.DMA((9,)),
        pltpu.SemaphoreType.DMA((6,)),
        pltpu.SemaphoreType.DMA((6,)),
    ]
    return pl.pallas_call(
        functools.partial(fused_kernel, ep_size, tp_size),
        name="fused_layer",
        out_shape=(
            jax.ShapeDtypeStruct(tokens.shape, BF16),
            jax.ShapeDtypeStruct((1, key_cache.shape[2]), BF16),
            jax.ShapeDtypeStruct((1, value_cache.shape[2]), BF16),
        ),
        in_specs=[vmem, vmem, hbm, hbm, hbm, hbm, hbm, smem, smem, vmem, hbm, vmem, smem, smem]
        + [hbm] * 3,
        out_specs=(vmem, vmem, vmem),
        scratch_shapes=scratch,
        compiler_params=pltpu.CompilerParams(
            collective_id=0, has_side_effects=True, vmem_limit_bytes=60 * 1024 * 1024
        ),
    )(
        tokens,
        norm_gain.reshape(1, -1),
        w_query,
        w_key,
        w_value,
        key_cache,
        value_cache,
        lengths,
        diff_lambda,
        head_gain.reshape(1, -1),
        w_out,
        ffn_gain.reshape(1, -1),
        routing,
        route_weight,
        w_gate,
        w_up,
        w_down,
    )


def layer(*arrays):
    tokens, w_query, w_key = arrays[0], arrays[2], arrays[3]
    feat = tokens.shape[1] // lax.axis_size("ep")
    whole_tiles = (
        tokens.shape[0] == 1
        and w_key.shape[1] == LANES
        and w_query.shape[1] == 8 * LANES
        and feat == 2 * LANES
        and tokens.shape[1] == 16 * LANES
    )
    return fused_body(*arrays) if whole_tiles else body(*arrays)


def solution(mesh):
    placed = (
        P(("ep", "tp"), None),
        P(),
        P("ep", "tp"),
        P("ep", "tp"),
        P("ep", "tp"),
        P(("ep", "tp"), None, None),
        P(("ep", "tp"), None, None),
        P(("ep", "tp")),
        P(),
        P(),
        P("tp", "ep"),
        P(),
        P("ep", None),
        P("ep", None),
        P("ep", None, "tp"),
        P("ep", None, "tp"),
        P("ep", "tp", None),
    )
    return jax.shard_map(
        layer,
        mesh=mesh,
        in_specs=placed,
        out_specs=(P(("ep", "tp"), None), P(("ep", "tp"), None), P(("ep", "tp"), None)),
        check_vma=False,
    )
```

profile of v0, /device:TPU:0, one launch (start us, length us, event | category | flops | bytes accessed | tf_op | source)
XLA Modules:
  0.0 47.0 jit_solution(4751556563043383788)
XLA Ops:
  1.3 1.3 %copy.20.routing_ref = s32[4,2]{1,0:T(4,128)} copy(s32[4,2]{0,1:T(2,128)} %param.29) | data formatting | bytes 64 | tf_op args[12]
  2.6 1.3 %copy.21.rweight_ref = f32[4,2]{1,0:T(4,128)} copy(f32[4,2]{0,1:T(2,128)} %param.30) | data formatting | bytes 64 | tf_op args[13]
  3.9 39.3 %fused_layer.1 = (bf16[1,2048]{1,0:T(2,128)(2,1)}, bf16[1,512]{1,0:T(2,128)(2,1)}, bf16[1,512]{1,0:T(2,128)(2,1)}) custom-call(bf16[1,2048]{1,0:T(2,128)(2,1)} %tok_ref.1, f32[1,2048]{1,0:T(1,128)} %bitcast.3, bf16[256,1024]{1,0:T(8,128)(2,1)} %wq_hbm.1, bf16[256,128]{1,0:T(8,128)(2,1)} %wk_hbm.1, bf16[256,128]{1,0:T(8,128)(2,1)} %wv_hbm.1, ...), custom_call_target="tpu_custom_call" | custom-call | tf_op jit(solution)/shard_map/fused_layer/pallas_call | solution.py:491
  43.2 1.3 %copy.26 = bf16[1,2048]{1,0:T(2,128)(2,1)} copy(bf16[1,2048]{1,0:T(2,128)(2,1)} %get-tuple-element.6) | data formatting | bytes 8192
  44.5 1.2 %copy.27 = bf16[1,512]{1,0:T(2,128)(2,1)} copy(bf16[1,512]{1,0:T(2,128)(2,1)} %get-tuple-element.7) | data formatting | bytes 2048
  45.8 1.2 %copy.28 = bf16[1,512]{1,0:T(2,128)(2,1)} copy(bf16[1,512]{1,0:T(2,128)(2,1)} %get-tuple-element.8) | data formatting | bytes 2048
where the time goes:
time: 47.3 us; the launch traced here: 47 us
  Pallas kernels  39.3 us (83%)
  local copies, waits for them, and re-layouts  6.46 us (14%)
  between operations  1.29 us (3%)
    pallas_call x1, Pallas kernels, fused_body(): pl.pallas_call(functools.partial(fused_kernel, ep_size, tp_size), name='f...  39.3 us
    unnamed x5, local copies, waits for them, and re-layouts  6.46 us

commit v1 on v0

--- a/solution.py
+++ b/solution.py
@@ -161,26 +161,33 @@
 def fused_kernel(
     ep_size,
     tp_size,
-    tok_ref,
-    norm_gain_ref,
+    tok_hbm,
+    norm_gain_hbm,
     wq_hbm,
     wk_hbm,
     wv_hbm,
     kc_hbm,
     vc_hbm,
-    len_ref,
-    lam_ref,
-    head_gain_ref,
+    len_s,
+    lam_hbm,
+    head_gain_hbm,
     wo_hbm,
-    ffn_gain_ref,
-    routing_ref,
-    rweight_ref,
+    ffn_gain_hbm,
+    routing_hbm,
+    rweight_hbm,
     wg_hbm,
     wu_hbm,
     wd_hbm,
     out_ref,
     nk_ref,
     nv_ref,
+    tok_v,
+    norm_gain,
+    head_gain,
+    ffn_gain,
+    lam_s,
+    routing_s,
+    rweight_s,
     wqkv,
     kc,
     vc,
@@ -194,116 +201,159 @@
     b_recv,
     c_send,
     c_recv,
-    d_send,
-    d_recv,
     r_send,
     r_recv,
     e_send,
     e_recv,
     stage,
     raw_keep,
-    res_stage,
+    gate_acc,
+    up_acc,
     load_sems,
     send_sems,
     recv_sems,
+    block_sems,
+    wo_send_sems,
+    wo_recv_sems,
 ):
     n_dev = ep_size * tp_size
     my_ep = lax.axis_index("ep")
     my_tp = lax.axis_index("tp")
     me = my_ep * tp_size + my_tp
-    width = tok_ref.shape[1]
+    width = tok_v.shape[1]
     feat = width // ep_size
     pieces = feat // LANES
     q_cols = wq_hbm.shape[1]
     q_rows = q_cols // LANES
     repeat = HEADS // KV_HEADS
-
-    loads = [
+    tile_rows = width // LANES
+    seq_ep = ep_size
+
+    def flips(index, size):
+        bits = [lax.rem(index // (1 << b), 2) for b in range(size.bit_length() - 1)]
+        return [
+            sum(
+                ((1 - bit) if (mask >> b) & 1 else bit) * (1 << b)
+                for b, bit in enumerate(bits)
+            )
+            for mask in range(size)
+        ]
+
+    ep_of = flips(my_ep, ep_size)
+    tp_of = flips(my_tp, tp_size)
+    everyone = [
+        (i, j) for i in reversed(range(ep_size)) for j in reversed(range(tp_size)) if i or j
+    ]
+    ep_peers = [(i, 0) for i in reversed(range(1, ep_size))]
+
+    barrier = pltpu.get_barrier_semaphore()
+    for i, j in everyone:
+        pl.semaphore_signal(
+            barrier,
+            inc=1,
+            device_id={"ep": ep_of[i], "tp": tp_of[j]},
+            device_id_type=pl.DeviceIdType.MESH,
+        )
+
+    rows_half = wo_hbm.shape[0] // 2
+    load_list = [
+        (tok_hbm, tok_v),
+        (norm_gain_hbm, norm_gain),
         (wq_hbm, wqkv.at[:, pl.ds(0, q_cols)]),
         (wk_hbm, wqkv.at[:, pl.ds(q_cols, LANES)]),
         (wv_hbm, wqkv.at[:, pl.ds(q_cols + LANES, LANES)]),
         (kc_hbm.at[0], kc),
         (vc_hbm.at[0], vc),
-        (wo_hbm, wo),
+        (lam_hbm, lam_s),
+        (head_gain_hbm, head_gain),
+        (wo_hbm, wo.at[my_tp]),
+        (ffn_gain_hbm, ffn_gain),
+        (routing_hbm, routing_s),
+        (rweight_hbm, rweight_s),
         (wg_hbm.at[0], wg),
         (wu_hbm.at[0], wu),
         (wd_hbm.at[0], wd),
     ]
     loads = [
-        pltpu.make_async_copy(src, dst, load_sems.at[i]) for i, (src, dst) in enumerate(loads)
+        pltpu.make_async_copy(src, dst, load_sems.at[i]) for i, (src, dst) in enumerate(load_list)
     ]
     for load in loads:
         load.start()
 
-    barrier = pltpu.get_barrier_semaphore()
-
-    def greet(step, carry):
-        to = lax.rem(me + step, n_dev)
-        pl.semaphore_signal(
-            barrier,
-            inc=1,
-            device_id={"ep": to // tp_size, "tp": lax.rem(to, tp_size)},
+    def ship(src, dst, i, j, send_sem, recv_sem):
+        copy = pltpu.make_async_remote_copy(
+            src_ref=src,
+            dst_ref=dst,
+            send_sem=send_sem,
+            recv_sem=recv_sem,
+            device_id={"ep": ep_of[i], "tp": tp_of[j]},
             device_id_type=pl.DeviceIdType.MESH,
         )
-        return carry
-
-    lax.fori_loop(1, n_dev, greet, 0)
-
-    def exchange(phase, count, source_of, target, place, device_of, my_place):
-        own = pltpu.make_async_copy(source_of(my_place), target.at[place], recv_sems.at[phase])
-        own.start()
-
-        def send(step, carry):
-            to = lax.rem(my_place + step, count)
-            pltpu.make_async_remote_copy(
-                src_ref=source_of(to),
-                dst_ref=target.at[place],
-                send_sem=send_sems.at[phase],
-                recv_sem=recv_sems.at[phase],
-                device_id=device_of(to),
-                device_id_type=pl.DeviceIdType.MESH,
-            ).start()
-            return carry
-
-        lax.fori_loop(1, count, send, 0)
-
-    def arrive(phase, target):
-        pltpu.make_async_copy(target, target, recv_sems.at[phase]).wait()
-
-    def flushed(phase, count, target):
-        part = target.at[pl.ds(0, count - 1)]
-        pltpu.make_async_copy(part, part, send_sems.at[phase]).wait()
-
-    def any_device(to):
-        return {"ep": to // tp_size, "tp": lax.rem(to, tp_size)}
-
-    tok = tok_ref[...].astype(F32)
+        copy.start()
+        return copy
+
+    def arrive(target, sem):
+        pltpu.make_async_copy(target, target, sem).wait()
+
+    loads[0].wait()
+    loads[1].wait()
+    tok = tok_v[...].astype(F32)
     mean_sq = jnp.mean(tok * tok, axis=-1, keepdims=True)
-    normed = tok * lax.rsqrt(mean_sq + NORM_EPS) * norm_gain_ref[...]
+    normed = tok * lax.rsqrt(mean_sq + NORM_EPS) * norm_gain[...]
     for e in range(ep_size):
         for p in range(pieces):
             cols = slice(e * feat + p * LANES, e * feat + (p + 1) * LANES)
             stage[e * 8 + p : e * 8 + p + 1, :] = normed[:, cols]
             stage[e * 8 + pieces + p : e * 8 + pieces + p + 1, :] = tok[:, cols]
     a_send[...] = stage[0 : ep_size * 8, :].astype(BF16).reshape(ep_size, 8, LANES)
+    a_recv[me] = a_send[my_ep]
     pl.semaphore_wait(barrier, n_dev - 1)
-    exchange(0, n_dev, lambda to: a_send.at[to // tp_size], a_recv, me, any_device, me)
-    arrive(0, a_recv)
+    for i, j in everyone:
+        ship(a_send.at[ep_of[i]], a_recv.at[me], i, j, send_sems.at[0], recv_sems.at[0])
+    wo_ships = [
+        ship(
+            wo_hbm.at[pl.ds(0, rows_half)],
+            wo.at[my_tp, pl.ds(0, rows_half)],
+            0,
+            2,
+            wo_send_sems.at[0],
+            wo_recv_sems.at[0],
+        )
+    ]
+    arrive(a_recv.at[pl.ds(0, n_dev - 1)], recv_sems.at[0])
     stage[0 : n_dev * 8, :] = a_recv[...].astype(F32).reshape(n_dev * 8, LANES)
     blocks = jnp.concatenate(
         [stage[pl.ds(p, n_dev, stride=8), :] for p in range(pieces)], axis=1
     ).astype(BF16)
     for p in range(pieces):
-        raw_keep[:, p * LANES : (p + 1) * LANES] = stage[pl.ds(pieces + p, n_dev, stride=8), :]
-
-    for i in range(3):
+        raw_keep[:, p * LANES : (p + 1) * LANES] = stage[
+            pl.ds(my_tp * 8 + pieces + p, ep_size, stride=8 * tp_size), :
+        ]
+
+    for i in range(2, 5):
         loads[i].wait()
     proj = jnp.dot(blocks, wqkv[...], preferred_element_type=F32)
     for j in range(q_rows + 2):
         stage[pl.ds(j, n_dev, stride=16), :] = proj[:, j * LANES : (j + 1) * LANES]
     b_send[...] = stage[...].astype(BF16).reshape(n_dev, 16, LANES)
-    exchange(1, n_dev, lambda to: b_send.at[to], b_recv, me, any_device, me)
-    arrive(1, b_recv)
+    for i, j in everyone:
+        to = ep_of[i] * tp_size + tp_of[j]
+        ship(b_send.at[to], b_recv.at[me], i, j, send_sems.at[1], recv_sems.at[1])
+    wo_ships.append(
+        ship(
+            wo_hbm.at[pl.ds(rows_half, rows_half)],
+            wo.at[my_tp, pl.ds(rows_half, rows_half)],
+            0,
+            2,
+            wo_send_sems.at[1],
+            wo_recv_sems.at[1],
+        )
+    )
+    b_recv[me] = b_send[me]
+    arrive(b_recv.at[pl.ds(0, n_dev - 1)], recv_sems.at[1])
+    wo_ships.append(
+        ship(wo_hbm, wo.at[my_tp], 0, 1, wo_send_sems.at[2], wo_recv_sems.at[2])
+    )
     q_parts, k_parts, v_parts = [], [], []
     for t in range(tp_size):
         total = b_recv[t].astype(F32)
@@ -318,10 +368,10 @@
         v_parts.append(value_row.astype(F32))
     q_all = jnp.concatenate(q_parts, axis=0).astype(BF16)
 
-    loads[3].wait()
-    loads[4].wait()
+    for i in range(5, 9):
+        loads[i].wait()
     rows = 2 * repeat
-    length = len_ref[0]
+    length = len_s[0]
     positions = kc.shape[0]
     first_map = lax.rem(lax.broadcasted_iota(jnp.int32, (rows, LANES), 0), 2) == 0
     first_wide = lax.rem(lax.broadcasted_iota(jnp.int32, (rows, positions), 0), 2) == 0
@@ -351,7 +401,7 @@
         own_weight = jnp.broadcast_to(own_weight / norm, (rows, LANES))
         lam = jnp.zeros((rows, LANES), F32)
         for r in range(repeat):
-            lam = jnp.where(head_at == r, lam_ref[g * repeat + r], lam)
+            lam = jnp.where(head_at == r, lam_s[g * repeat + r], lam)
         mix = (weight - lam[:, 0:1] * pltpu.roll(weight, rows - 1, 0)).astype(BF16)
         mix_own = (own_weight - lam * pltpu.roll(own_weight, rows - 1, 0)).astype(BF16).astype(F32)
         raw = jnp.dot(
@@ -361,76 +411,120 @@
             [mix_own * v_parts[2 * g], mix_own * v_parts[2 * g + 1]], axis=1
         )
         mean_sq = jnp.mean(raw * raw, axis=-1, keepdims=True)
-        head = raw * lax.rsqrt(mean_sq + HEAD_EPS) * head_gain_ref[...] * HEAD_SCALE
-        for half in range(2):
-            at = half * KV_HEADS * rows + g * rows
-            stage[at : at + rows, :] = head[:, half * LANES : (half + 1) * LANES]
-    heads_dev = HEADS // tp_size
-    halves = [stage[pl.ds(half * KV_HEADS * rows, HEADS, stride=2), :] for half in range(2)]
-    for t in range(tp_size):
-        for half in range(2):
-            at = t * 8 + half * heads_dev
-            stage[at : at + heads_dev, :] = halves[half][t * heads_dev : (t + 1) * heads_dev]
-    c_send[...] = stage[0 : tp_size * 8, :].astype(BF16).reshape(tp_size, 8, LANES)
-    exchange(2, n_dev, lambda to: c_send.at[lax.rem(to, tp_size)], c_recv, me, any_device, me)
-    arrive(2, c_recv)
-
-    stage[0 : n_dev * 8, :] = c_recv[...].astype(F32).reshape(n_dev * 8, LANES)
+        head = raw * lax.rsqrt(mean_sq + HEAD_EPS) * head_gain[...] * HEAD_SCALE
+        c_send[g * rows : (g + 1) * rows, :] = jnp.where(
+            first_map, head[:, 0:LANES], pltpu.roll(head[:, LANES : 2 * LANES], 1, 0)
+        ).astype(BF16)
+    for i, j in ep_peers:
+        ship(c_send, c_recv.at[my_ep], i, j, send_sems.at[2], recv_sems.at[2])
+    c_recv[my_ep] = c_send[...]
+    for half in range(2):
+        block = wo.at[tp_of[2], pl.ds(half * rows_half, rows_half)]
+        arrive(block, wo_recv_sems.at[half])
+        wo_ships.append(
+            ship(block, block, 0, 1, wo_send_sems.at[3 + half], wo_recv_sems.at[3 + half])
+        )
+    loads[9].wait()
+    arrive(wo.at[tp_of[1]], wo_recv_sems.at[2])
+    for half in range(2):
+        block = wo.at[tp_of[3], pl.ds(half * rows_half, rows_half)]
+        arrive(block, wo_recv_sems.at[3 + half])
+    loads[10].wait()
+    arrive(c_recv.at[pl.ds(0, ep_size - 1)], recv_sems.at[2])
+
+    head_rows = c_send.shape[0]
+    stage[0 : seq_ep * head_rows, :] = c_recv[...].astype(F32).reshape(seq_ep * head_rows, LANES)
     lhs = jnp.concatenate(
-        [
-            stage[pl.ds(half * heads_dev + r, n_dev, stride=8), :]
-            for r in range(heads_dev)
-            for half in range(2)
-        ],
-        axis=1,
+        [stage[pl.ds(r, seq_ep, stride=head_rows), :] for r in range(head_rows)], axis=1
     ).astype(BF16)
-    loads[5].wait()
-    d_send[...] = jnp.dot(lhs, wo[...], preferred_element_type=F32).astype(BF16)
-    exchange(3, tp_size, lambda to: d_send, d_recv, my_tp, lambda to: {"tp": to}, my_tp)
-    arrive(3, d_recv)
+    k_block = wo.shape[1]
     total = raw_keep[...]
     for t in range(tp_size):
-        total = total + d_recv[t].astype(F32)
+        total = total + jnp.dot(
+            lhs[:, t * k_block : (t + 1) * k_block], wo[t], preferred_element_type=F32
+        )
     r_send[...] = total.astype(BF16)
-    exchange(4, ep_size, lambda to: r_send, r_recv, my_ep, lambda to: {"ep": to}, my_ep)
-    arrive(4, r_recv)
-    residual = jnp.concatenate([r_recv[e].astype(F32) for e in range(ep_size)], axis=1)
-    tile_rows = width // LANES
-    for j in range(tile_rows):
-        res_stage[pl.ds(j, n_dev, stride=tile_rows), :] = residual[:, j * LANES : (j + 1) * LANES]
-    mean_sq = jnp.mean(residual * residual, axis=-1, keepdims=True)
-    ffn_in = (residual * lax.rsqrt(mean_sq + NORM_EPS) * ffn_gain_ref[...]).astype(BF16)
-
-    loads[6].wait()
-    gate = jnp.dot(ffn_in, wg[...], preferred_element_type=F32)
-    loads[7].wait()
-    up = jnp.dot(ffn_in, wu[...], preferred_element_type=F32)
+    for i, j in everyone:
+        ship(r_send, r_recv.at[my_ep, my_tp], i, j, send_sems.at[3], block_sems.at[i // 2])
+    r_recv[my_ep, my_tp] = r_send[...]
+
+    loads[13].wait()
+    loads[14].wait()
+    square = jnp.zeros((n_dev, LANES), F32)
+    for k in range(ep_size // 2):
+        arrive(e_recv.at[pl.ds(0, 2 * tp_size if k else 2 * tp_size - 1)], block_sems.at[k])
+        gate_add = None
+        for i in (2 * k, 2 * k + 1):
+            at = pl.multiple_of(ep_of[i] * feat, feat)
+            block = r_recv[ep_of[i]].astype(F32).reshape(n_dev, feat)
+            for p in range(pieces):
+                part = block[:, p * LANES : (p + 1) * LANES]
+                square = square + part * part
+            scaled = (block * ffn_gain[:, pl.ds(at, feat)]).astype(BF16)
+            g_part = jnp.dot(scaled, wg[pl.ds(at, feat), :], preferred_element_type=F32)
+            u_part = jnp.dot(scaled, wu[pl.ds(at, feat), :], preferred_element_type=F32)
+            gate_add = g_part if gate_add is None else gate_add + g_part
+            up_add = u_part if i == 2 * k else up_add + u_part
+        if k == 0:
+            gate_acc[...] = gate_add
+            up_acc[...] = up_add
+        elif k < ep_size // 2 - 1:
+            gate_acc[...] += gate_add
+            up_acc[...] += up_add
+    row_scale = lax.rsqrt(jnp.sum(square, axis=-1, keepdims=True) * (1.0 / width) + NORM_EPS)
+    gate = (gate_acc[...] + gate_add) * row_scale
+    up = (up_acc[...] + up_add) * row_scale
     hidden = (gate / (1.0 + jnp.exp(-gate)) * up).astype(BF16)
-    loads[8].wait()
+    loads[15].wait()
     down = jnp.dot(hidden, wd[...], preferred_element_type=F32)
     for j in range(tile_rows):
         stage[pl.ds(j, n_dev, stride=tile_rows), :] = down[:, j * LANES : (j + 1) * LANES]
-    e_send[...] = stage[...].astype(BF16).reshape(n_dev, tile_rows, LANES)
-    exchange(5, n_dev, lambda to: e_send.at[to], e_recv, me, any_device, me)
-    arrive(5, e_recv)
-    result = res_stage[pl.ds(me * tile_rows, tile_rows), :]
+    e_send[...] = stage[...].astype(BF16).reshape(tp_size, ep_size, tile_rows, LANES)
+    for i, j in everyone:
+        ship(
+            e_send.at[tp_of[j], ep_of[i]], e_recv.at[me], i, j, send_sems.at[4], recv_sems.at[3]
+        )
+    e_recv[me] = e_send[my_tp, my_ep]
+    loads[11].wait()
+    loads[12].wait()
+    own_rows = []
+    for e in range(ep_size):
+        for p in range(pieces):
+            own_rows.append((e, p))
+    for e, p in own_rows:
+        block = r_recv[e, my_tp].astype(F32)
+        stage[e * 8 : e * 8 + 8, :] = block[:, 0:LANES]
+        stage[(ep_size + e) * 8 : (ep_size + e) * 8 + 8, :] = block[:, LANES : 2 * LANES]
+    result = [
+        stage[pl.ds((half * ep_size) * 8 + my_ep, ep_size, stride=8), :] for half in range(pieces)
+    ]
+    for half in range(pieces):
+        stage[pl.ds(256 + half, ep_size, stride=pieces), :] = result[half]
+    result = stage[256 : 256 + tile_rows, :]
+    shares = []
     for e in range(ep_size):
         share = jnp.float32(0.0)
         for k in range(TOPK):
-            share = share + jnp.where(routing_ref[my_tp, k] == e, rweight_ref[my_tp, k], 0.0)
+            share = share + jnp.where(routing_s[k, my_tp] == e, rweight_s[k, my_tp], 0.0)
+        shares.append(share)
+    for ship_done in wo_ships:
+        ship_done.wait_send()
+    for phase, part in (
+        (0, a_recv.at[pl.ds(0, n_dev - 1)]),
+        (1, b_recv.at[pl.ds(0, n_dev - 1)]),
+        (2, c_recv.at[pl.ds(0, ep_size - 1)]),
+    ):
+        arrive(part, send_sems.at[phase])
+    arrive(e_recv.at[pl.ds(0, n_dev - 1)], send_sems.at[3])
+    arrive(e_recv.at[pl.ds(0, n_dev - 1)], recv_sems.at[3])
+    for e in range(ep_size):
         total = e_recv[e * tp_size].astype(F32)
         for t in range(1, tp_size):
             total = total + e_recv[e * tp_size + t].astype(F32)
-        result = result + total.astype(BF16).astype(F32) * share
+        result = result + total.astype(BF16).astype(F32) * shares[e]
     for j in range(tile_rows):
         out_ref[:, j * LANES : (j + 1) * LANES] = result[j : j + 1].astype(BF16)
-
-    flushed(0, n_dev, a_recv)
-    flushed(1, n_dev, b_recv)
-    flushed(2, n_dev, c_recv)
-    flushed(3, tp_size, d_recv)
-    flushed(4, ep_size, r_recv)
-    flushed(5, n_dev, e_recv)
+    arrive(e_recv.at[pl.ds(0, n_dev - 1)], send_sems.at[4])
 
 
 def fused_body(
@@ -457,15 +551,22 @@
     width = tokens.shape[1]
     feat = width // ep_size
     vmem = pl.BlockSpec(memory_space=pltpu.VMEM)
-    smem = pl.BlockSpec(memory_space=pltpu.SMEM)
-    hbm = pl.BlockSpec(memory_space=pl.ANY)
+    hbm = pl.BlockSpec(memory_space=pltpu.HBM)
     tile_rows = width // LANES
     proj_cols = w_query.shape[1] + w_key.shape[1] + w_value.shape[1]
+    head_tiles = HEADS * HEAD_V // LANES
     scratch = [
+        pltpu.VMEM(tokens.shape, BF16),
+        pltpu.VMEM((1, width), F32),
+        pltpu.VMEM((1, HEAD_V), F32),
+        pltpu.VMEM((1, width), F32),
+        pltpu.SMEM(diff_lambda.shape, F32),
+        pltpu.SMEM(routing.shape[::-1], jnp.int32),
+        pltpu.SMEM(route_weight.shape[::-1], F32),
         pltpu.VMEM((feat, proj_cols), BF16),
         pltpu.VMEM(key_cache.shape[1:], BF16),
         pltpu.VMEM(value_cache.shape[1:], BF16),
-        pltpu.VMEM(w_out.shape, BF16),
+        pltpu.VMEM((tp_size,) + w_out.shape, BF16),
         pltpu.VMEM(w_gate.shape[1:], BF16),
         pltpu.VMEM(w_up.shape[1:], BF16),
         pltpu.VMEM(w_down.shape[1:], BF16),
@@ -473,22 +574,24 @@
         pltpu.VMEM((n_dev, 8, LANES), BF16),
         pltpu.VMEM((n_dev, 16, LANES), BF16),
         pltpu.VMEM((n_dev, 16, LANES), BF16),
-        pltpu.VMEM((tp_size, 8, LANES), BF16),
-        pltpu.VMEM((n_dev, 8, LANES), BF16),
-        pltpu.VMEM((n_dev, feat), BF16),
-        pltpu.VMEM((tp_size, n_dev, feat), BF16),
-        pltpu.VMEM((n_dev, feat), BF16),
-        pltpu.VMEM((ep_size, n_dev, feat), BF16),
-        pltpu.VMEM((n_dev, tile_rows, LANES), BF16),
+        pltpu.VMEM((head_tiles, LANES), BF16),
+        pltpu.VMEM((ep_size, head_tiles, LANES), BF16),
+        pltpu.VMEM((ep_size, feat), BF16),
+        pltpu.VMEM((ep_size, tp_size, ep_size, feat), BF16),
+        pltpu.VMEM((tp_size, ep_size, tile_rows, LANES), BF16),
         pltpu.VMEM((n_dev, tile_rows, LANES), BF16),
         pltpu.VMEM((n_dev * 16, LANES), F32),
-        pltpu.VMEM((n_dev, feat), F32),
-        pltpu.VMEM((n_dev * tile_rows, LANES), F32),
-        pltpu.SemaphoreType.DMA((9,)),
-        pltpu.SemaphoreType.DMA((6,)),
-        pltpu.SemaphoreType.DMA((6,)),
+        pltpu.VMEM((ep_size, feat), F32),
+        pltpu.VMEM((n_dev, w_gate.shape[2]), F32),
+        pltpu.VMEM((n_dev, w_gate.shape[2]), F32),
+        pltpu.SemaphoreType.DMA((16,)),
+        pltpu.SemaphoreType.DMA((5,)),
+        pltpu.SemaphoreType.DMA((4,)),
+        pltpu.SemaphoreType.DMA((ep_size // 2,)),
+        pltpu.SemaphoreType.DMA((5,)),
+        pltpu.SemaphoreType.DMA((5,)),
     ]
-    return pl.pallas_call(
+    call = pl.pallas_call(
         functools.partial(fused_kernel, ep_size, tp_size),
         name="fused_layer",
         out_shape=(
@@ -496,14 +599,14 @@
             jax.ShapeDtypeStruct((1, key_cache.shape[2]), BF16),
             jax.ShapeDtypeStruct((1, value_cache.shape[2]), BF16),
         ),
-        in_specs=[vmem, vmem, hbm, hbm, hbm, hbm, hbm, smem, smem, vmem, hbm, vmem, smem, smem]
-        + [hbm] * 3,
+        in_specs=[hbm] * 7 + [pl.BlockSpec(memory_space=pltpu.SMEM)] + [hbm] * 9,
         out_specs=(vmem, vmem, vmem),
         scratch_shapes=scratch,
         compiler_params=pltpu.CompilerParams(
-            collective_id=0, has_side_effects=True, vmem_limit_bytes=60 * 1024 * 1024
+            collective_id=0, has_side_effects=True, vmem_limit_bytes=28 * 1024 * 1024
         ),
-    )(
+    )
+    operands = (
         tokens,
         norm_gain.reshape(1, -1),
         w_query,
@@ -516,12 +619,17 @@
         head_gain.reshape(1, -1),
         w_out,
         ffn_gain.reshape(1, -1),
-        routing,
-        route_weight,
+        routing.T,
+        route_weight.T,
         w_gate,
         w_up,
         w_down,
     )
+    pinned = [
+        array if array is lengths else pltpu.with_memory_space_constraint(array, pltpu.HBM)
+        for array in operands
+    ]
+    return call(*pinned)
 
 
 def layer(*arrays):

time: 47.3 us -> 39.6 us (0.84)
  local copies, waits for them, and re-layouts: 6.46 us -> 1.76 us
  Pallas kernels: 39.3 us -> 36.4 us
    unnamed x5 -> x3, local copies, waits for them, and re-layouts: 6.46 us -> 1.76 us
    pallas_call x1, Pallas kernels: 39.3 us -> 36.4 us  [fused_body(): return call(*pinned)]
where the time goes in v1:
time: 39.6 us; the launch traced here: 39.4 us
  Pallas kernels  36.4 us (92%)
  local copies, waits for them, and re-layouts  1.76 us (4%)
  between operations  1.29 us (3%)
    pallas_call x1, Pallas kernels, fused_body(): return call(*pinned)  36.4 us
    unnamed x3, local copies, waits for them, and re-layouts  1.76 us

profile of v1, /device:TPU:0, one launch (start us, length us, event | category | flops | bytes accessed | tf_op | source)
XLA Modules:
  0.0 39.4 jit_solution(4819716821578579239)
XLA Ops:
  1.3 36.4 %fused_layer.1 = (bf16[1,2048]{1,0:T(2,128)(2,1)S(1)}, bf16[1,512]{1,0:T(2,128)(2,1)S(1)}, bf16[1,512]{1,0:T(2,128)(2,1)S(1)}) custom-call(bf16[1,2048]{1,0:T(2,128)(2,1)} %tok_hbm.1, f32[1,2048]{1,0:T(1,128)} %bitcast.5, bf16[256,1024]{1,0:T(8,128)(2,1)} %wq_hbm.1, bf16[256,128]{1,0:T(8,128)(2,1)} %wk_hbm.1, bf16[256,128]{1,0:T(8,128)(2,1)} %wv_hbm.1, ...), custom_call_target="tpu_custom_call" | custom-call | tf_op jit(solution)/shard_map/fused_layer/pallas_call | solution.py:632
  37.7 0.6 %copy.24 = bf16[1,2048]{1,0:T(2,128)(2,1)} copy(bf16[1,2048]{1,0:T(2,128)(2,1)S(1)} %get-tuple-element.6) | data formatting | bytes 8192
  38.3 0.6 %copy.25 = bf16[1,512]{1,0:T(2,128)(2,1)} copy(bf16[1,512]{1,0:T(2,128)(2,1)S(1)} %get-tuple-element.7) | data formatting | bytes 2048
  38.8 0.6 %copy.26 = bf16[1,512]{1,0:T(2,128)(2,1)} copy(bf16[1,512]{1,0:T(2,128)(2,1)S(1)} %get-tuple-element.8) | data formatting | bytes 2048

commit v2 on v1

--- a/solution.py
+++ b/solution.py
@@ -156,6 +156,10 @@
 F32 = jnp.float32
 BF16 = jnp.bfloat16
 LANES = 128
+
+
+WO_CUTS = (4, 4)
+WO_FIRST = 1
 
 
 def fused_kernel(
@@ -190,6 +194,7 @@
     rweight_s,
     wqkv,
     kc,
+    kt,
     vc,
     wo,
     wg,
@@ -220,6 +225,10 @@
     my_ep = lax.axis_index("ep")
     my_tp = lax.axis_index("tp")
     me = my_ep * tp_size + my_tp
+    my_row, my_col = my_tp // 2, lax.rem(my_tp, 2)
+    other_col = 1 - my_col
+    my_slot = my_ep * 2 + my_row
+    slots = 2 * ep_size
     width = tok_v.shape[1]
     feat = width // ep_size
     pieces = feat // LANES
@@ -227,7 +236,9 @@
     q_rows = q_cols // LANES
     repeat = HEADS // KV_HEADS
     tile_rows = width // LANES
-    seq_ep = ep_size
+    a_rows = a_send.shape[1]
+    b_tiles, b_rows = b_send.shape[1:3]
+    b_span = b_tiles * b_rows
 
     def flips(index, size):
         bits = [lax.rem(index // (1 << b), 2) for b in range(size.bit_length() - 1)]
@@ -244,7 +255,8 @@
     everyone = [
         (i, j) for i in reversed(range(ep_size)) for j in reversed(range(tp_size)) if i or j
     ]
-    ep_peers = [(i, 0) for i in reversed(range(1, ep_size))]
+    spread = sorted(everyone, key=lambda peer: -((peer[0] // 2) ^ (peer[0] // 4)))
+    cross = [(i, j) for i in reversed(range(ep_size)) for j in (3, 1)]
 
     barrier = pltpu.get_barrier_semaphore()
     for i, j in everyone:
@@ -255,18 +267,42 @@
             device_id_type=pl.DeviceIdType.MESH,
         )
 
-    rows_half = wo_hbm.shape[0] // 2
+    wo_rows = wo_hbm.shape[0]
+    near_cols = pl.ds(pl.multiple_of(my_row * LANES, LANES), LANES)
+    far_cols = pl.ds(pl.multiple_of((1 - my_row) * LANES, LANES), LANES)
+    cuts = [wo_rows * eighths // 8 for eighths in WO_CUTS]
+    spans = [pl.ds(sum(cuts[:n]), count) for n, count in enumerate(cuts)]
+    wo_ships = []
+
+    def wo_push(n):
+        wo_ships.append(
+            ship(
+                wo_hbm.at[spans[n], far_cols],
+                wo.at[my_tp, spans[n]],
+                0,
+                2,
+                wo_send_sems.at[n],
+                wo_recv_sems.at[n],
+            )
+        )
+
+    def wo_forward(n):
+        at = len(cuts) + 1 + n
+        block = wo.at[tp_of[2], spans[n]]
+        arrive(block, wo_recv_sems.at[n])
+        wo_ships.append(ship(block, block, 0, 1, wo_send_sems.at[at], wo_recv_sems.at[at]))
+
     load_list = [
         (tok_hbm, tok_v),
         (norm_gain_hbm, norm_gain),
-        (wq_hbm, wqkv.at[:, pl.ds(0, q_cols)]),
-        (wk_hbm, wqkv.at[:, pl.ds(q_cols, LANES)]),
-        (wv_hbm, wqkv.at[:, pl.ds(q_cols + LANES, LANES)]),
+        (wq_hbm, wqkv.at[my_col, :, pl.ds(0, q_cols)]),
+        (wk_hbm, wqkv.at[my_col, :, pl.ds(q_cols, LANES)]),
+        (wv_hbm, wqkv.at[my_col, :, pl.ds(q_cols + LANES, LANES)]),
         (kc_hbm.at[0], kc),
         (vc_hbm.at[0], vc),
         (lam_hbm, lam_s),
         (head_gain_hbm, head_gain),
-        (wo_hbm, wo.at[my_tp]),
+        (wo_hbm.at[:, near_cols], wo.at[my_tp]),
         (ffn_gain_hbm, ffn_gain),
         (routing_hbm, routing_s),
         (rweight_hbm, rweight_s),
@@ -303,93 +339,110 @@
     for e in range(ep_size):
         for p in range(pieces):
             cols = slice(e * feat + p * LANES, e * feat + (p + 1) * LANES)
-            stage[e * 8 + p : e * 8 + p + 1, :] = normed[:, cols]
-            stage[e * 8 + pieces + p : e * 8 + pieces + p + 1, :] = tok[:, cols]
-    a_send[...] = stage[0 : ep_size * 8, :].astype(BF16).reshape(ep_size, 8, LANES)
-    a_recv[me] = a_send[my_ep]
+            at = e * a_rows + p
+            stage[at : at + 1, :] = normed[:, cols]
+            stage[at + pieces : at + pieces + 1, :] = tok[:, cols]
+    for e in range(ep_size):
+        a_send[e] = stage[e * a_rows : (e + 1) * a_rows, :].astype(BF16)
     pl.semaphore_wait(barrier, n_dev - 1)
-    for i, j in everyone:
-        ship(a_send.at[ep_of[i]], a_recv.at[me], i, j, send_sems.at[0], recv_sems.at[0])
-    wo_ships = [
+    for i, j in cross:
+        ship(a_send.at[ep_of[i]], a_recv.at[my_slot], i, j, send_sems.at[0], recv_sems.at[0])
+    pair_ships = [
         ship(
-            wo_hbm.at[pl.ds(0, rows_half)],
-            wo.at[my_tp, pl.ds(0, rows_half)],
+            src,
+            wqkv.at[my_col, :, pl.ds(first, src.shape[1])],
             0,
-            2,
-            wo_send_sems.at[0],
-            wo_recv_sems.at[0],
+            1,
+            wo_send_sems.at[2 * len(cuts) + 1 + n],
+            wo_recv_sems.at[2 * len(cuts) + 1 + n],
+        )
+        for n, (src, first) in enumerate(
+            ((wq_hbm, 0), (wk_hbm, q_cols), (wv_hbm, q_cols + LANES))
         )
     ]
-    arrive(a_recv.at[pl.ds(0, n_dev - 1)], recv_sems.at[0])
-    stage[0 : n_dev * 8, :] = a_recv[...].astype(F32).reshape(n_dev * 8, LANES)
+    for n in range(WO_FIRST):
+        wo_push(n)
+    arrive(a_recv, recv_sems.at[0])
+    for n in range(slots):
+        stage[n * a_rows : (n + 1) * a_rows, :] = a_recv[n].astype(F32)
     blocks = jnp.concatenate(
-        [stage[pl.ds(p, n_dev, stride=8), :] for p in range(pieces)], axis=1
+        [stage[pl.ds(p, slots, stride=a_rows), :] for p in range(pieces)], axis=1
     ).astype(BF16)
-    for p in range(pieces):
-        raw_keep[:, p * LANES : (p + 1) * LANES] = stage[
-            pl.ds(my_tp * 8 + pieces + p, ep_size, stride=8 * tp_size), :
-        ]
+    raw_keep[...] = stage[pl.ds(pieces + my_row, slots, stride=a_rows), :]
 
     for i in range(2, 5):
         loads[i].wait()
-    proj = jnp.dot(blocks, wqkv[...], preferred_element_type=F32)
-    for j in range(q_rows + 2):
-        stage[pl.ds(j, n_dev, stride=16), :] = proj[:, j * LANES : (j + 1) * LANES]
-    b_send[...] = stage[...].astype(BF16).reshape(n_dev, 16, LANES)
-    for i, j in everyone:
-        to = ep_of[i] * tp_size + tp_of[j]
-        ship(b_send.at[to], b_recv.at[me], i, j, send_sems.at[1], recv_sems.at[1])
+    for n, (first, count) in enumerate(((0, q_cols), (q_cols, LANES), (q_cols + LANES, LANES))):
+        arrive(
+            wqkv.at[other_col, :, pl.ds(first, count)], wo_recv_sems.at[2 * len(cuts) + 1 + n]
+        )
+    for col in range(2):
+        proj = jnp.dot(blocks, wqkv[col], preferred_element_type=F32)
+        rows_at = [col * q_rows + j for j in range(q_rows)] + [2 * q_rows + col, 2 * q_rows + 2 + col]
+        for j, at in enumerate(rows_at):
+            stage[pl.ds(at, slots, stride=b_span), :] = proj[:, j * LANES : (j + 1) * LANES]
+    for n in range(slots):
+        for k in range(b_tiles):
+            at = n * b_span + k * b_rows
+            b_send[n, k] = stage[at : at + b_rows, :].astype(BF16)
+    for i, j in cross:
+        to = ep_of[i] * 2 + tp_of[j] // 2
+        ship(b_send.at[to], b_recv.at[my_slot], i, j, send_sems.at[1], recv_sems.at[1])
+    for n in range(WO_FIRST, len(cuts)):
+        wo_push(n)
     wo_ships.append(
         ship(
-            wo_hbm.at[pl.ds(rows_half, rows_half)],
-            wo.at[my_tp, pl.ds(rows_half, rows_half)],
+            wo_hbm.at[:, near_cols],
+            wo.at[my_tp],
             0,
-            2,
-            wo_send_sems.at[1],
-            wo_recv_sems.at[1],
-        )
-    )
-    b_recv[me] = b_send[me]
-    arrive(b_recv.at[pl.ds(0, n_dev - 1)], recv_sems.at[1])
-    wo_ships.append(
-        ship(wo_hbm, wo.at[my_tp], 0, 1, wo_send_sems.at[2], wo_recv_sems.at[2])
-    )
-    q_parts, k_parts, v_parts = [], [], []
-    for t in range(tp_size):
-        total = b_recv[t].astype(F32)
+            1,
+            wo_send_sems.at[len(cuts)],
+            wo_recv_sems.at[len(cuts)],
+        )
+    )
+    loads[5].wait()
+    for part in range(kc.shape[1] // HEAD_QK):
+        cols = slice(part * HEAD_QK, (part + 1) * HEAD_QK)
+        kt[cols, :] = kc[:, cols].T
+    arrive(b_recv, recv_sems.at[1])
+    for n in range(WO_FIRST):
+        wo_forward(n)
+    k_parts, v_parts = [], []
+    for row in range(2):
+        total = b_recv[row].astype(F32)
         for e in range(1, ep_size):
-            total = total + b_recv[e * tp_size + t].astype(F32)
-        q_parts.append(total[0:q_rows])
-        key_row = total[q_rows : q_rows + 1].astype(BF16)
-        value_row = total[q_rows + 1 : q_rows + 2].astype(BF16)
-        nk_ref[:, t * LANES : (t + 1) * LANES] = key_row
-        nv_ref[:, t * LANES : (t + 1) * LANES] = value_row
-        k_parts.append(key_row.astype(F32))
-        v_parts.append(value_row.astype(F32))
-    q_all = jnp.concatenate(q_parts, axis=0).astype(BF16)
-
-    for i in range(5, 9):
+            total = total + b_recv[e * 2 + row].astype(F32)
+        for k in range(2 * q_rows // b_rows):
+            at = row * 2 * q_rows + k * b_rows
+            stage[at : at + b_rows, :] = total[k]
+        for col in range(2):
+            t = row * 2 + col
+            key_row = total[b_tiles - 1, col : col + 1].astype(BF16)
+            value_row = total[b_tiles - 1, 2 + col : 3 + col].astype(BF16)
+            nk_ref[:, t * LANES : (t + 1) * LANES] = key_row
+            nv_ref[:, t * LANES : (t + 1) * LANES] = value_row
+            k_parts.append(key_row.astype(F32))
+            v_parts.append(value_row.astype(F32))
+    q_all = stage[0 : tp_size * q_rows, :].astype(BF16)
+
+    for i in range(6, 9):
         loads[i].wait()
     rows = 2 * repeat
     length = len_s[0]
     positions = kc.shape[0]
     first_map = lax.rem(lax.broadcasted_iota(jnp.int32, (rows, LANES), 0), 2) == 0
-    first_wide = lax.rem(lax.broadcasted_iota(jnp.int32, (rows, positions), 0), 2) == 0
     valid = lax.broadcasted_iota(jnp.int32, (rows, positions), 1) < length
     head_at = lax.broadcasted_iota(jnp.int32, (rows, LANES), 0) // 2
     scale = HEAD_QK ** (-0.5)
-    contract = (((1,), (1,)), ((), ()))
     for g in range(KV_HEADS):
         q = q_all[g * rows : (g + 1) * rows]
         base = g * 2 * HEAD_QK
-        s0 = lax.dot_general(
-            q, kc[:, base : base + HEAD_QK], contract, preferred_element_type=F32
-        )
-        s1 = lax.dot_general(
-            q, kc[:, base + HEAD_QK : base + 2 * HEAD_QK], contract, preferred_element_type=F32
-        )
-        score = jnp.where(valid, jnp.where(first_wide, s0, s1) * scale, -jnp.inf)
         q32 = q.astype(F32)
+        both = jnp.concatenate(
+            [jnp.where(first_map, q32, 0.0), jnp.where(first_map, 0.0, q32)], axis=1
+        ).astype(BF16)
+        score = jnp.dot(both, kt[base : base + 2 * HEAD_QK, :], preferred_element_type=F32)
+        score = jnp.where(valid, score * scale, -jnp.inf)
         own = jnp.sum(
             q32 * jnp.where(first_map, k_parts[2 * g], k_parts[2 * g + 1]), axis=-1, keepdims=True
         ) * scale
@@ -415,60 +468,67 @@
         c_send[g * rows : (g + 1) * rows, :] = jnp.where(
             first_map, head[:, 0:LANES], pltpu.roll(head[:, LANES : 2 * LANES], 1, 0)
         ).astype(BF16)
-    for i, j in ep_peers:
-        ship(c_send, c_recv.at[my_ep], i, j, send_sems.at[2], recv_sems.at[2])
-    c_recv[my_ep] = c_send[...]
-    for half in range(2):
-        block = wo.at[tp_of[2], pl.ds(half * rows_half, rows_half)]
-        arrive(block, wo_recv_sems.at[half])
-        wo_ships.append(
-            ship(block, block, 0, 1, wo_send_sems.at[3 + half], wo_recv_sems.at[3 + half])
-        )
+    for i, j in cross:
+        ship(c_send, c_recv.at[my_slot], i, j, send_sems.at[2], recv_sems.at[2])
+    for n in range(WO_FIRST, len(cuts)):
+        wo_forward(n)
     loads[9].wait()
-    arrive(wo.at[tp_of[1]], wo_recv_sems.at[2])
-    for half in range(2):
-        block = wo.at[tp_of[3], pl.ds(half * rows_half, rows_half)]
-        arrive(block, wo_recv_sems.at[3 + half])
     loads[10].wait()
-    arrive(c_recv.at[pl.ds(0, ep_size - 1)], recv_sems.at[2])
+    arrive(wo.at[tp_of[1]], wo_recv_sems.at[len(cuts)])
+    for n in range(len(cuts)):
+        arrive(wo.at[tp_of[3], spans[n]], wo_recv_sems.at[len(cuts) + 1 + n])
+    arrive(c_recv, recv_sems.at[2])
 
     head_rows = c_send.shape[0]
-    stage[0 : seq_ep * head_rows, :] = c_recv[...].astype(F32).reshape(seq_ep * head_rows, LANES)
-    lhs = jnp.concatenate(
-        [stage[pl.ds(r, seq_ep, stride=head_rows), :] for r in range(head_rows)], axis=1
-    ).astype(BF16)
-    k_block = wo.shape[1]
+    tiles_block = head_rows // tp_size
+    for n in range(slots):
+        part = c_recv[n].astype(F32)
+        for t in range(tp_size):
+            at = (t * slots + n) * tiles_block
+            stage[at : at + tiles_block, :] = part[t * tiles_block : (t + 1) * tiles_block]
+
     total = raw_keep[...]
     for t in range(tp_size):
-        total = total + jnp.dot(
-            lhs[:, t * k_block : (t + 1) * k_block], wo[t], preferred_element_type=F32
-        )
+        lhs = jnp.concatenate(
+            [
+                stage[pl.ds(t * tiles_block * slots + r, slots, stride=tiles_block), :]
+                for r in range(tiles_block)
+            ],
+            axis=1,
+        ).astype(BF16)
+        total = total + jnp.dot(lhs, wo[t], preferred_element_type=F32)
     r_send[...] = total.astype(BF16)
-    for i, j in everyone:
-        ship(r_send, r_recv.at[my_ep, my_tp], i, j, send_sems.at[3], block_sems.at[i // 2])
+    for i, j in spread:
+        ship(r_send, r_recv.at[my_ep, my_tp], i, j, send_sems.at[3], block_sems.at[i])
     r_recv[my_ep, my_tp] = r_send[...]
 
     loads[13].wait()
     loads[14].wait()
+    low, high = lax.rem(my_ep // 2, 2), my_ep // 4
+    inner = low + high - 2 * low * high
+    order = [(at_end, inside) for at_end, inside in zip((1, 0, 3, 2, 5, 4, 7, 6), (1, 0, 7, 6, 3, 2, 5, 4))]
+
+    def pick(at_end, inside):
+        return inside * inner + at_end * (1 - inner)
+
     square = jnp.zeros((n_dev, LANES), F32)
-    for k in range(ep_size // 2):
-        arrive(e_recv.at[pl.ds(0, 2 * tp_size if k else 2 * tp_size - 1)], block_sems.at[k])
-        gate_add = None
-        for i in (2 * k, 2 * k + 1):
-            at = pl.multiple_of(ep_of[i] * feat, feat)
-            block = r_recv[ep_of[i]].astype(F32).reshape(n_dev, feat)
-            for p in range(pieces):
-                part = block[:, p * LANES : (p + 1) * LANES]
-                square = square + part * part
-            scaled = (block * ffn_gain[:, pl.ds(at, feat)]).astype(BF16)
-            g_part = jnp.dot(scaled, wg[pl.ds(at, feat), :], preferred_element_type=F32)
-            u_part = jnp.dot(scaled, wu[pl.ds(at, feat), :], preferred_element_type=F32)
-            gate_add = g_part if gate_add is None else gate_add + g_part
-            up_add = u_part if i == 2 * k else up_add + u_part
-        if k == 0:
+    for step, (at_end, inside) in enumerate(order):
+        place = pick(ep_of[at_end], ep_of[inside])
+        count = tp_size if at_end else tp_size - 1
+        arrive(r_recv.at[place, pl.ds(0, count)], block_sems.at[pick(at_end, inside)])
+        at = pl.multiple_of(place * feat, feat)
+        parts = []
+        for p in range(pieces):
+            part = r_recv[place, 2 * p : 2 * p + 2].astype(F32).reshape(n_dev, LANES)
+            square = square + part * part
+            parts.append(part * ffn_gain[:, pl.ds(at + p * LANES, LANES)])
+        scaled = jnp.concatenate(parts, axis=1).astype(BF16)
+        gate_add = jnp.dot(scaled, wg[pl.ds(at, feat), :], preferred_element_type=F32)
+        up_add = jnp.dot(scaled, wu[pl.ds(at, feat), :], preferred_element_type=F32)
+        if step == 0:
             gate_acc[...] = gate_add
             up_acc[...] = up_add
-        elif k < ep_size // 2 - 1:
+        elif step < ep_size - 1:
             gate_acc[...] += gate_add
             up_acc[...] += up_add
     row_scale = lax.rsqrt(jnp.sum(square, axis=-1, keepdims=True) * (1.0 / width) + NORM_EPS)
@@ -476,43 +536,43 @@
     up = (up_acc[...] + up_add) * row_scale
     hidden = (gate / (1.0 + jnp.exp(-gate)) * up).astype(BF16)
     loads[15].wait()
+
+    def row_of(e, t):
+        return (1 - lax.rem(t, 2)) * slots + e * 2 + t // 2
+
     down = jnp.dot(hidden, wd[...], preferred_element_type=F32)
     for j in range(tile_rows):
         stage[pl.ds(j, n_dev, stride=tile_rows), :] = down[:, j * LANES : (j + 1) * LANES]
-    e_send[...] = stage[...].astype(BF16).reshape(tp_size, ep_size, tile_rows, LANES)
-    for i, j in everyone:
+    e_send[...] = stage[...].astype(BF16).reshape(n_dev, tile_rows, LANES)
+    for i, j in spread:
         ship(
-            e_send.at[tp_of[j], ep_of[i]], e_recv.at[me], i, j, send_sems.at[4], recv_sems.at[3]
-        )
-    e_recv[me] = e_send[my_tp, my_ep]
+            e_send.at[row_of(ep_of[i], tp_of[j])],
+            e_recv.at[me],
+            i,
+            j,
+            send_sems.at[4],
+            recv_sems.at[3],
+        )
+    e_recv[me] = e_send[row_of(my_ep, my_tp)]
     loads[11].wait()
     loads[12].wait()
-    own_rows = []
     for e in range(ep_size):
         for p in range(pieces):
-            own_rows.append((e, p))
-    for e, p in own_rows:
-        block = r_recv[e, my_tp].astype(F32)
-        stage[e * 8 : e * 8 + 8, :] = block[:, 0:LANES]
-        stage[(ep_size + e) * 8 : (ep_size + e) * 8 + 8, :] = block[:, LANES : 2 * LANES]
-    result = [
-        stage[pl.ds((half * ep_size) * 8 + my_ep, ep_size, stride=8), :] for half in range(pieces)
-    ]
-    for half in range(pieces):
-        stage[pl.ds(256 + half, ep_size, stride=pieces), :] = result[half]
-    result = stage[256 : 256 + tile_rows, :]
+            at = (e * pieces + p) * slots
+            stage[at : at + slots, :] = r_recv[e, 2 * p + other_col].astype(F32)
+    result = stage[pl.ds(my_slot, tile_rows, stride=slots), :]
     shares = []
     for e in range(ep_size):
         share = jnp.float32(0.0)
         for k in range(TOPK):
             share = share + jnp.where(routing_s[k, my_tp] == e, rweight_s[k, my_tp], 0.0)
         shares.append(share)
-    for ship_done in wo_ships:
+    for ship_done in wo_ships + pair_ships:
         ship_done.wait_send()
     for phase, part in (
-        (0, a_recv.at[pl.ds(0, n_dev - 1)]),
-        (1, b_recv.at[pl.ds(0, n_dev - 1)]),
-        (2, c_recv.at[pl.ds(0, ep_size - 1)]),
+        (0, a_recv),
+        (1, b_recv),
+        (2, c_recv),
     ):
         arrive(part, send_sems.at[phase])
     arrive(e_recv.at[pl.ds(0, n_dev - 1)], send_sems.at[3])
@@ -525,6 +585,19 @@
     for j in range(tile_rows):
         out_ref[:, j * LANES : (j + 1) * LANES] = result[j : j + 1].astype(BF16)
     arrive(e_recv.at[pl.ds(0, n_dev - 1)], send_sems.at[4])
+
+
+def write_kernel(result_ref, keys_ref, values_ref, result_out, keys_out, values_out, sems):
+    copies = [
+        pltpu.make_async_copy(src, dst, sems.at[i])
+        for i, (src, dst) in enumerate(
+            ((result_ref, result_out), (keys_ref, keys_out), (values_ref, values_out))
+        )
+    ]
+    for copy in copies:
+        copy.start()
+    for copy in copies:
+        copy.wait()
 
 
 def fused_body(
@@ -563,33 +636,34 @@
         pltpu.SMEM(diff_lambda.shape, F32),
         pltpu.SMEM(routing.shape[::-1], jnp.int32),
         pltpu.SMEM(route_weight.shape[::-1], F32),
-        pltpu.VMEM((feat, proj_cols), BF16),
+        pltpu.VMEM((2, feat, proj_cols), BF16),
         pltpu.VMEM(key_cache.shape[1:], BF16),
+        pltpu.VMEM(key_cache.shape[:0:-1], BF16),
         pltpu.VMEM(value_cache.shape[1:], BF16),
-        pltpu.VMEM((tp_size,) + w_out.shape, BF16),
+        pltpu.VMEM((tp_size, w_out.shape[0], LANES), BF16),
         pltpu.VMEM(w_gate.shape[1:], BF16),
         pltpu.VMEM(w_up.shape[1:], BF16),
         pltpu.VMEM(w_down.shape[1:], BF16),
-        pltpu.VMEM((ep_size, 8, LANES), BF16),
-        pltpu.VMEM((n_dev, 8, LANES), BF16),
-        pltpu.VMEM((n_dev, 16, LANES), BF16),
-        pltpu.VMEM((n_dev, 16, LANES), BF16),
+        pltpu.VMEM((ep_size, 4, LANES), BF16),
+        pltpu.VMEM((2 * ep_size, 4, LANES), BF16),
+        pltpu.VMEM((2 * ep_size, 5, 4, LANES), BF16),
+        pltpu.VMEM((2 * ep_size, 5, 4, LANES), BF16),
         pltpu.VMEM((head_tiles, LANES), BF16),
-        pltpu.VMEM((ep_size, head_tiles, LANES), BF16),
-        pltpu.VMEM((ep_size, feat), BF16),
-        pltpu.VMEM((ep_size, tp_size, ep_size, feat), BF16),
-        pltpu.VMEM((tp_size, ep_size, tile_rows, LANES), BF16),
+        pltpu.VMEM((2 * ep_size, head_tiles, LANES), BF16),
+        pltpu.VMEM((2 * ep_size, LANES), BF16),
+        pltpu.VMEM((ep_size, tp_size, 2 * ep_size, LANES), BF16),
+        pltpu.VMEM((n_dev, tile_rows, LANES), BF16),
         pltpu.VMEM((n_dev, tile_rows, LANES), BF16),
         pltpu.VMEM((n_dev * 16, LANES), F32),
-        pltpu.VMEM((ep_size, feat), F32),
+        pltpu.VMEM((2 * ep_size, LANES), F32),
         pltpu.VMEM((n_dev, w_gate.shape[2]), F32),
         pltpu.VMEM((n_dev, w_gate.shape[2]), F32),
         pltpu.SemaphoreType.DMA((16,)),
         pltpu.SemaphoreType.DMA((5,)),
         pltpu.SemaphoreType.DMA((4,)),
-        pltpu.SemaphoreType.DMA((ep_size // 2,)),
-        pltpu.SemaphoreType.DMA((5,)),
-        pltpu.SemaphoreType.DMA((5,)),
+        pltpu.SemaphoreType.DMA((ep_size,)),
+        pltpu.SemaphoreType.DMA((2 * len(WO_CUTS) + 4,)),
+        pltpu.SemaphoreType.DMA((2 * len(WO_CUTS) + 4,)),
     ]
     call = pl.pallas_call(
         functools.partial(fused_kernel, ep_size, tp_size),
@@ -629,7 +703,16 @@
         array if array is lengths else pltpu.with_memory_space_constraint(array, pltpu.HBM)
         for array in operands
     ]
-    return call(*pinned)
+    made = call(*pinned)
+    return pl.pallas_call(
+        write_kernel,
+        name="write_out",
+        out_shape=tuple(jax.ShapeDtypeStruct(array.shape, array.dtype) for array in made),
+        in_specs=[vmem] * len(made),
+        out_specs=tuple(pl.BlockSpec(memory_space=pl.ANY) for _ in made),
+        scratch_shapes=[pltpu.SemaphoreType.DMA((len(made),))],
+        compiler_params=pltpu.CompilerParams(vmem_limit_bytes=1024 * 1024),
+    )(*made)
 
 
 def layer(*arrays):

time: 39.6 us -> 35.6 us (0.90)
  Pallas kernels: 36.4 us -> 34 us
  local copies, waits for them, and re-layouts: 1.76 us -> 0 us
    pallas_call x1 -> x2, Pallas kernels: 36.4 us -> 34 us  [the longest x1 33.4 us: fused_body(): made = call(*pinned)]
    unnamed x3 -> x0, local copies, waits for them, and re-layouts: 1.76 us -> none
where the time goes in v2:
time: 35.6 us; the launch traced here: 35.3 us
  Pallas kernels  34 us (96%)
  between operations  1.29 us (4%)
    pallas_call x1, Pallas kernels, fused_body(): made = call(*pinned)  33.4 us

profile of v2, /device:TPU:0, one launch (start us, length us, event | category | flops | bytes accessed | tf_op | source)
XLA Modules:
  0.0 35.3 jit_solution(2508064882577178789)
XLA Ops:
  1.3 33.4 %fused_layer.1 = (bf16[1,2048]{1,0:T(2,128)(2,1)S(1)}, bf16[1,512]{1,0:T(2,128)(2,1)S(1)}, bf16[1,512]{1,0:T(2,128)(2,1)S(1)}) custom-call(bf16[1,2048]{1,0:T(2,128)(2,1)} %tok_hbm.1, f32[1,2048]{1,0:T(1,128)} %bitcast.5, bf16[256,1024]{1,0:T(8,128)(2,1)} %wq_hbm.1, bf16[256,128]{1,0:T(8,128)(2,1)} %wk_hbm.1, bf16[256,128]{1,0:T(8,128)(2,1)} %wv_hbm.1, ...), custom_call_target="tpu_custom_call" | custom-call | tf_op jit(solution)/shard_map/fused_layer/pallas_call | solution.py:706
  34.7 0.6 %write_out.1 = (bf16[1,2048]{1,0:T(2,128)(2,1)}, bf16[1,512]{1,0:T(2,128)(2,1)}, bf16[1,512]{1,0:T(2,128)(2,1)}) custom-call(bf16[1,2048]{1,0:T(2,128)(2,1)S(1)} %get-tuple-element.6.result_ref, bf16[1,512]{1,0:T(2,128)(2,1)S(1)} %get-tuple-element.7.keys_ref, bf16[1,512]{1,0:T(2,128)(2,1)S(1)} %get-tuple-element.8.values_ref), custom_call_target="tpu_custom_call" | custom-call | tf_op jit(solution)/shard_map/write_out/pallas_call | solution.py:707

commit v3 on v2

--- a/solution.py
+++ b/solution.py
@@ -158,7 +158,7 @@
 LANES = 128
 
 
-WO_CUTS = (4, 4)
+WO_CUTS = (6, 2)
 WO_FIRST = 1
 
 
@@ -255,8 +255,14 @@
     everyone = [
         (i, j) for i in reversed(range(ep_size)) for j in reversed(range(tp_size)) if i or j
     ]
-    spread = sorted(everyone, key=lambda peer: -((peer[0] // 2) ^ (peer[0] // 4)))
-    cross = [(i, j) for i in reversed(range(ep_size)) for j in (3, 1)]
+    row_to = (my_row, 1 - my_row)
+    targets = [
+        (i, row_to[flip] * 2 + col)
+        for col in range(2)
+        for flip in (1, 0)
+        for i in reversed(range(1, ep_size))
+    ] + [(0, tp_of[j]) for j in reversed(range(1, tp_size))]
+    cross = [(i, j) for j in (3, 1) for i in reversed(range(ep_size))]
 
     barrier = pltpu.get_barrier_semaphore()
     for i, j in everyone:
@@ -316,17 +322,20 @@
     for load in loads:
         load.start()
 
-    def ship(src, dst, i, j, send_sem, recv_sem):
+    def ship_to(src, dst, i, to, send_sem, recv_sem):
         copy = pltpu.make_async_remote_copy(
             src_ref=src,
             dst_ref=dst,
             send_sem=send_sem,
             recv_sem=recv_sem,
-            device_id={"ep": ep_of[i], "tp": tp_of[j]},
+            device_id={"ep": ep_of[i], "tp": to},
             device_id_type=pl.DeviceIdType.MESH,
         )
         copy.start()
         return copy
+
+    def ship(src, dst, i, j, send_sem, recv_sem):
+        return ship_to(src, dst, i, tp_of[j], send_sem, recv_sem)
 
     def arrive(target, sem):
         pltpu.make_async_copy(target, target, sem).wait()
@@ -404,6 +413,20 @@
     for part in range(kc.shape[1] // HEAD_QK):
         cols = slice(part * HEAD_QK, (part + 1) * HEAD_QK)
         kt[cols, :] = kc[:, cols].T
+    for i in range(6, 9):
+        loads[i].wait()
+    rows = 2 * repeat
+    length = len_s[0]
+    positions = kc.shape[0]
+    first_map = lax.rem(lax.broadcasted_iota(jnp.int32, (rows, LANES), 0), 2) == 0
+    valid = lax.broadcasted_iota(jnp.int32, (rows, positions), 1) < length
+    head_at = lax.broadcasted_iota(jnp.int32, (rows, LANES), 0) // 2
+    lams = []
+    for g in range(KV_HEADS):
+        lam = jnp.zeros((rows, LANES), F32)
+        for r in range(repeat):
+            lam = jnp.where(head_at == r, lam_s[g * repeat + r], lam)
+        lams.append(lam)
     arrive(b_recv, recv_sems.at[1])
     for n in range(WO_FIRST):
         wo_forward(n)
@@ -425,41 +448,41 @@
             v_parts.append(value_row.astype(F32))
     q_all = stage[0 : tp_size * q_rows, :].astype(BF16)
 
-    for i in range(6, 9):
-        loads[i].wait()
-    rows = 2 * repeat
-    length = len_s[0]
-    positions = kc.shape[0]
-    first_map = lax.rem(lax.broadcasted_iota(jnp.int32, (rows, LANES), 0), 2) == 0
-    valid = lax.broadcasted_iota(jnp.int32, (rows, positions), 1) < length
-    head_at = lax.broadcasted_iota(jnp.int32, (rows, LANES), 0) // 2
     scale = HEAD_QK ** (-0.5)
+    scores, owns = [], []
     for g in range(KV_HEADS):
-        q = q_all[g * rows : (g + 1) * rows]
+        q32 = q_all[g * rows : (g + 1) * rows].astype(F32)
         base = g * 2 * HEAD_QK
-        q32 = q.astype(F32)
         both = jnp.concatenate(
             [jnp.where(first_map, q32, 0.0), jnp.where(first_map, 0.0, q32)], axis=1
         ).astype(BF16)
         score = jnp.dot(both, kt[base : base + 2 * HEAD_QK, :], preferred_element_type=F32)
-        score = jnp.where(valid, score * scale, -jnp.inf)
-        own = jnp.sum(
-            q32 * jnp.where(first_map, k_parts[2 * g], k_parts[2 * g + 1]), axis=-1, keepdims=True
-        ) * scale
+        scores.append(jnp.where(valid, score * scale, -jnp.inf))
+        owns.append(
+            jnp.sum(
+                q32 * jnp.where(first_map, k_parts[2 * g], k_parts[2 * g + 1]),
+                axis=-1,
+                keepdims=True,
+            )
+            * scale
+        )
+    mixes, mixes_own = [], []
+    for score, own, lam in zip(scores, owns, lams):
         peak = jnp.maximum(jnp.max(score, axis=-1, keepdims=True), own)
         weight = jnp.exp(score - peak)
         own_weight = jnp.exp(own - peak)
         norm = jnp.sum(weight, axis=-1, keepdims=True) + own_weight
         weight = weight / norm
         own_weight = jnp.broadcast_to(own_weight / norm, (rows, LANES))
-        lam = jnp.zeros((rows, LANES), F32)
-        for r in range(repeat):
-            lam = jnp.where(head_at == r, lam_s[g * repeat + r], lam)
-        mix = (weight - lam[:, 0:1] * pltpu.roll(weight, rows - 1, 0)).astype(BF16)
-        mix_own = (own_weight - lam * pltpu.roll(own_weight, rows - 1, 0)).astype(BF16).astype(F32)
-        raw = jnp.dot(
-            mix, vc[:, g * HEAD_V : (g + 1) * HEAD_V], preferred_element_type=F32
-        )
+        mixes.append((weight - lam[:, 0:1] * pltpu.roll(weight, rows - 1, 0)).astype(BF16))
+        mixes_own.append(
+            (own_weight - lam * pltpu.roll(own_weight, rows - 1, 0)).astype(BF16).astype(F32)
+        )
+    raws = [
+        jnp.dot(mix, vc[:, g * HEAD_V : (g + 1) * HEAD_V], preferred_element_type=F32)
+        for g, mix in enumerate(mixes)
+    ]
+    for g, (raw, mix_own) in enumerate(zip(raws, mixes_own)):
         raw = raw + jnp.concatenate(
             [mix_own * v_parts[2 * g], mix_own * v_parts[2 * g + 1]], axis=1
         )
@@ -498,15 +521,15 @@
         ).astype(BF16)
         total = total + jnp.dot(lhs, wo[t], preferred_element_type=F32)
     r_send[...] = total.astype(BF16)
-    for i, j in spread:
-        ship(r_send, r_recv.at[my_ep, my_tp], i, j, send_sems.at[3], block_sems.at[i])
+    for i, to in targets:
+        ship_to(r_send, r_recv.at[my_ep, my_tp], i, to, send_sems.at[3], block_sems.at[i])
     r_recv[my_ep, my_tp] = r_send[...]
 
     loads[13].wait()
     loads[14].wait()
     low, high = lax.rem(my_ep // 2, 2), my_ep // 4
     inner = low + high - 2 * low * high
-    order = [(at_end, inside) for at_end, inside in zip((1, 0, 3, 2, 5, 4, 7, 6), (1, 0, 7, 6, 3, 2, 5, 4))]
+    order = [(at_end, inside) for at_end, inside in zip((1, 0, 5, 4, 3, 2, 7, 6), (1, 0, 7, 6, 3, 2, 5, 4))]
 
     def pick(at_end, inside):
         return inside * inner + at_end * (1 - inner)
@@ -544,14 +567,9 @@
     for j in range(tile_rows):
         stage[pl.ds(j, n_dev, stride=tile_rows), :] = down[:, j * LANES : (j + 1) * LANES]
     e_send[...] = stage[...].astype(BF16).reshape(n_dev, tile_rows, LANES)
-    for i, j in spread:
-        ship(
-            e_send.at[row_of(ep_of[i], tp_of[j])],
-            e_recv.at[me],
-            i,
-            j,
-            send_sems.at[4],
-            recv_sems.at[3],
+    for i, to in targets:
+        ship_to(
+            e_send.at[row_of(ep_of[i], to)], e_recv.at[me], i, to, send_sems.at[4], recv_sems.at[3]
         )
     e_recv[me] = e_send[row_of(my_ep, my_tp)]
     loads[11].wait()

time: 35.6 us -> 34.5 us (0.969)
  Pallas kernels: 34 us -> 32.6 us
    pallas_call x1, Pallas kernels: 33.4 us -> 32 us  [fused_body(): made = call(*pinned)]
where the time goes in v3:
time: 34.5 us; the launch traced here: 33.9 us
  Pallas kernels  32.6 us (94%)
  between operations  1.29 us (4%)
    pallas_call x1, Pallas kernels, fused_body(): made = call(*pinned)  32 us

profile of v3, /device:TPU:0, one launch (start us, length us, event | category | flops | bytes accessed | tf_op | source)
XLA Modules:
  0.0 33.9 jit_solution(6060649626752422295)
XLA Ops:
  1.3 32.0 %fused_layer.1 = (bf16[1,2048]{1,0:T(2,128)(2,1)S(1)}, bf16[1,512]{1,0:T(2,128)(2,1)S(1)}, bf16[1,512]{1,0:T(2,128)(2,1)S(1)}) custom-call(bf16[1,2048]{1,0:T(2,128)(2,1)} %tok_hbm.1, f32[1,2048]{1,0:T(1,128)} %bitcast.5, bf16[256,1024]{1,0:T(8,128)(2,1)} %wq_hbm.1, bf16[256,128]{1,0:T(8,128)(2,1)} %wk_hbm.1, bf16[256,128]{1,0:T(8,128)(2,1)} %wv_hbm.1, ...), custom_call_target="tpu_custom_call" | custom-call | tf_op jit(solution)/shard_map/fused_layer/pallas_call | solution.py:724
  33.3 0.6 %write_out.1 = (bf16[1,2048]{1,0:T(2,128)(2,1)}, bf16[1,512]{1,0:T(2,128)(2,1)}, bf16[1,512]{1,0:T(2,128)(2,1)}) custom-call(bf16[1,2048]{1,0:T(2,128)(2,1)S(1)} %get-tuple-element.6.result_ref, bf16[1,512]{1,0:T(2,128)(2,1)S(1)} %get-tuple-element.7.keys_ref, bf16[1,512]{1,0:T(2,128)(2,1)S(1)} %get-tuple-element.8.values_ref), custom_call_target="tpu_custom_call" | custom-call | tf_op jit(solution)/shard_map/write_out/pallas_call | solution.py:725
